TPU v7x, 512 devices: a whole 4x4x16 slice. The times are simulated.
512 devices in a mesh: rep: 2 (over z_hi), fs: 32 (over z_lo, y), tp: 8 (over x, core).
Axes of the slice: x: 4, y: 4, z: 16 (z_hi: 2, z_lo: 8; z = z_hi * 8 + z_lo), core: 2. Of those that a mesh axis runs over, the one named last changes fastest.
Arguments:
- tokens_in: bfloat16 [16384, 2048], P(('rep', 'fs', 'tp')), may hold values from -6 to 6
- norm_gains: float32 [3, 2048], replicated, may hold values from 0.1 to 1.9
- gate_w: float32 [2048, 3072], P('fs', 'tp'), may hold values from -0.125 to 0.125
- gate_scale: float32 [3072], P('tp'), may hold values from 0.5 to 2
- up_w: float32 [2048, 3072], P('fs', 'tp'), may hold values from -0.125 to 0.125
- up_scale: float32 [3072], P('tp'), may hold values from 0.5 to 2
- down_w: float32 [3072, 2048], P('tp', 'fs'), may hold values from -0.109375 to 0.109375
- down_scale: float32 [2048], P('fs'), may hold values from 0.5 to 2
- query_w: float32 [2048, 2048], P('fs', 'tp'), may hold values from -0.125 to 0.125
- query_scale: float32 [2048], P('tp'), may hold values from 0.5 to 2
- key_w: float32 [2048, 2048], P('fs', 'tp'), may hold values from -0.125 to 0.125
- key_scale: float32 [2048], P('tp'), may hold values from 0.5 to 2
- value_w: float32 [2048, 2048], P('fs', 'tp'), may hold values from -0.125 to 0.125
- value_scale: float32 [2048], P('tp'), may hold values from 0.5 to 2
- out_w: float32 [2048, 2048], P('tp', 'fs'), may hold values from -0.125 to 0.125
- out_scale: float32 [2048], P('fs'), may hold values from 0.5 to 2
- head_gain: float32 [256], replicated, may hold values from 0.1 to 1.9
- decay_rate: float32 [8], P('tp'), may hold values from 0 to 1, as said below
Outputs:
- tokens_out: bfloat16 [16384, 2048], P(('rep', 'fs', 'tp'))
Inputs may be any that keep to these rules, and one draw needn't show every extreme that they name: `decay_rate`: each head's decay per position, positive.
All inputs are finite; a program needn't handle non-finite values.
Results may differ from a plain program's by a relative error of at most 0.02.
Values may be sent and summed in bfloat16 or wider, within the bound.
No kernel may reach another device: no remote copies, remote signals or barrier semaphores. Data moves between devices by JAX's collectives and lax.ppermute only.
A program may use at most 64 MiB of HBM per device.

v0:
```python
import math
import jax
import jax.numpy as jnp
from jax import lax
from jax.sharding import PartitionSpec as P

DK = 256
DV = 256
BLOCK = 64
EPSILON = 1e-05


def gather_turned(arrays, axis, dims):
    turned = [jnp.moveaxis(a, dim, 0) for a, dim in zip(arrays, dims)]
    widths = [t[0].size for t in turned]
    both = jnp.concatenate([t.reshape(-1, w) for t, w in zip(turned, widths)], axis=1)
    result = lax.all_gather(both, axis, axis=0, tiled=True)
    blocks = jnp.split(result, [sum(widths[:k]) for k in range(1, len(widths))], axis=1)
    return tuple(
        (
            jnp.moveaxis(b.reshape(-1, *t.shape[1:]), 0, dim)
            for b, t, dim in zip(blocks, turned, dims)
        )
    )


def sent_to_all(array, axis):
    copies = jnp.broadcast_to(array, (lax.axis_size(axis), *array.shape))
    return lax.all_to_all(copies, axis, split_axis=0, concat_axis=0, tiled=True)


def in_order(blocks, dim):
    shape = list(blocks.shape[1:])
    shape[dim] *= blocks.shape[0]
    return jnp.moveaxis(blocks, 0, dim).reshape(shape)


def collect(array, axis, dim):
    blocks = sent_to_all(array, axis)
    return in_order(blocks, dim)


def in_blocks(array, dim, devices):
    shape = array.shape
    blocks = array.reshape(*shape[:dim], devices, shape[dim] // devices, *shape[dim + 1 :])
    return jnp.moveaxis(blocks, dim, 0)


def summed_on_arrival(array, axis, dim):
    blocks = in_blocks(array, dim, lax.axis_size(axis))
    arrived = lax.all_to_all(blocks, axis, split_axis=0, concat_axis=0, tiled=True)
    return arrived.astype(jnp.float32).sum(axis=0)


def in_one_piece(arrays, axis, dim, along):
    both = jnp.concatenate(arrays, axis=along)
    result, at, finished = (lax.all_gather(both, axis, axis=dim, tiled=True), 0, [])
    for a in arrays:
        finished.append(lax.slice_in_dim(result, at, at + a.shape[along], axis=along))
        at += a.shape[along]
    return tuple(finished)


def rms_scale(stream, gain):
    return stream * lax.rsqrt(jnp.mean(stream * stream, axis=-1, keepdims=True) + EPSILON) * gain


def retain(query, key_rows, value, decay_rate, head_gain):
    seq_len = query.shape[0]
    blocks = seq_len // BLOCK
    local_heads = decay_rate.shape[0]
    q_heads = query.reshape(blocks, BLOCK, local_heads, DK).transpose(0, 2, 1, 3)
    k_heads = key_rows.reshape(blocks, BLOCK, local_heads, DK).transpose(0, 2, 1, 3)
    v_heads = value.reshape(blocks, BLOCK, local_heads, DV).transpose(0, 2, 1, 3)
    offsets = jnp.arange(BLOCK, dtype=jnp.float32)
    inner_decay = jnp.exp(-decay_rate[:, None, None] * jnp.abs(offsets[:, None] - offsets[None, :]))
    query_decay = jnp.exp(-decay_rate[:, None] * offsets[None, :])[..., None]
    key_decay = jnp.exp(-decay_rate[:, None] * (BLOCK - offsets)[None, :])[..., None]
    block_decay = jnp.exp(-decay_rate * BLOCK)[:, None, None]

    def advance(state, inputs):
        q_blk, k_blk, v_blk = inputs
        scores = (
            jnp.einsum("hid,hjd->hij", q_blk, k_blk, preferred_element_type=jnp.float32)
            * inner_decay
        )
        scores = scores.astype(jnp.bfloat16)
        within = jnp.einsum("hij,hje->hie", scores, v_blk, preferred_element_type=jnp.float32)
        carried = jnp.einsum(
            "hid,hde->hie",
            q_blk.astype(jnp.float32) * query_decay,
            state,
            precision=lax.Precision.HIGHEST,
        )
        k_weighted = k_blk.astype(jnp.float32) * key_decay
        state = state * block_decay + jnp.einsum(
            "hjd,hje->hde", k_weighted, v_blk.astype(jnp.float32), precision=lax.Precision.HIGHEST
        )
        return (state, within + carried)

    initial = jnp.zeros((local_heads, DK, DV), jnp.float32)
    _, retained = lax.scan(advance, initial, (q_heads, k_heads, v_heads))
    retained = retained.transpose(0, 2, 1, 3).reshape(seq_len, local_heads, DV)
    centred = retained - jnp.mean(retained, axis=-1, keepdims=True)
    normed = (
        centred
        * lax.rsqrt(jnp.mean(centred * centred, axis=-1, keepdims=True) + EPSILON)
        * head_gain
    )
    return normed.reshape(seq_len, local_heads * DV).astype(jnp.bfloat16)


def on_device(
    tokens_in,
    norm_gains,
    gate_w,
    gate_scale,
    up_w,
    up_scale,
    down_w,
    down_scale,
    query_w,
    query_scale,
    key_w,
    key_scale,
    value_w,
    value_scale,
    out_w,
    out_scale,
    head_gain,
    decay_rate,
):
    down_cols, out_cols = gather_turned((down_scale, out_scale), "fs", (0, 0))
    gate_b = gate_w.astype(jnp.bfloat16)
    up_b = up_w.astype(jnp.bfloat16)
    down_b = down_w.astype(jnp.bfloat16)
    query_b = query_w.astype(jnp.bfloat16)
    key_b = key_w.astype(jnp.bfloat16)
    value_b = value_w.astype(jnp.bfloat16)
    out_b = out_w.astype(jnp.bfloat16)

    def gather_rows(normed):
        return collect(normed, "tp", 0)

    def return_rows(hidden, weight, scale):
        return summed_on_arrival(
            (jnp.dot(hidden, weight, preferred_element_type=jnp.float32) * scale).astype(
                jnp.bfloat16
            ),
            "tp",
            0,
        )

    def feed_forward(stream, gain, weights):
        gate_full, up_full, down_full = weights
        gathered = gather_rows(rms_scale(stream, gain).astype(jnp.bfloat16))
        gate_value = jnp.dot(gathered, gate_full, preferred_element_type=jnp.float32) * gate_scale
        up_value = jnp.dot(gathered, up_full, preferred_element_type=jnp.float32) * up_scale
        hidden = (jax.nn.silu(gate_value) * up_value).astype(jnp.bfloat16)
        return return_rows(hidden, down_full, down_cols)

    stream = tokens_in.astype(jnp.float32)
    held = gather_turned((gate_b, up_b, down_b), "fs", (0, 0, 1))
    stream = stream + 0.5 * feed_forward(stream, norm_gains[0], held)
    gathered = gather_rows(rms_scale(stream, norm_gains[1]).astype(jnp.bfloat16))
    segments = in_one_piece((query_b, key_b, value_b), "fs", 0, 1)
    query_raw, key_raw, value_raw = tuple(
        (jnp.dot(gathered, segment_w, preferred_element_type=jnp.float32) for segment_w in segments)
    )
    out_full = collect(out_b, "fs", 1)
    query = (query_raw * query_scale).astype(jnp.bfloat16)
    key_rows = (key_raw * key_scale / math.sqrt(DK)).astype(jnp.bfloat16)
    value = (value_raw * value_scale).astype(jnp.bfloat16)
    mixed = retain(query, key_rows, value, decay_rate, head_gain)
    stream = stream + return_rows(mixed, out_full, out_cols)
    stream = stream + 0.5 * feed_forward(stream, norm_gains[2], held)
    return stream.astype(jnp.bfloat16)


def solution(mesh):
    placed = (
        P(("rep", "fs", "tp"), None),
        P(),
        P("fs", "tp"),
        P("tp"),
        P("fs", "tp"),
        P("tp"),
        P("tp", "fs"),
        P("fs"),
        P("fs", "tp"),
        P("tp"),
        P("fs", "tp"),
        P("tp"),
        P("fs", "tp"),
        P("tp"),
        P("tp", "fs"),
        P("fs"),
        P(),
        P("tp"),
    )
    return jax.shard_map(
        on_device,
        mesh=mesh,
        in_specs=placed,
        out_specs=P(("rep", "fs", "tp"), None),
        check_vma=False,
    )
```

profile of v0, /device:TPU:1, one launch (start us, length us, event | category | flops | bytes accessed | tf_op | source)
XLA Modules:
  0.0 551.2 jit_solution(16911982376912300465)
XLA Ops:
  6.5 0.9 convert_bitcast_fusion
  7.4 0.9 convert_element_type.138
  8.3 0.9 convert_element_type.139
  9.2 0.7 pad_maximum_fusion
  9.9 0.0 all-gather.4.cloned.1.call-update
  9.9 0.0 all-gather.6.cloned.1.call-start
  10.0 0.8 convert_element_type.145
  10.8 0.9 convert_element_type.146
  11.7 0.8 convert_element_type.147
  12.6 0.6 pad_maximum_fusion.1
  13.2 0.0 all-gather.6.cloned.1.call-update
  13.2 1.0 fusion.108
  14.3 0.9 fusion.124
  15.2 1.0 fusion.110
  16.2 1.2 broadcast_in_dim.17
  17.4 10.3 %all-to-all-start = ((bf16[8,32,2048]{2,1,0:T(8,128)(2,1)}), bf16[8,32,2048]{2,1,0:T(8,128)(2,1)S(1)}, u32[]{:S(2)}, u32[]{:S(2)}) async-start(bf16[8,32,2048]{2,1,0:T(8,128)(2,1)} %broadcast_in_dim.17), calls=%async_computation | async-start | bytes 2097152 | tf_op jit(solution)/shard_map/all_to_all | solution.py:29
  27.7 107.8 %all-gather = f32[32,64,2]{1,2,0:T(2,128)S(1)} all-gather(f32[1,64,2]{1,2,0:T(2,128)S(1)} %maximum_bitcast_fusion), channel_id=1, replica_groups=mesh['rep'=2,'fs'=32,'tp'=8] {'fs'}, dimensions={0}, use_global_device_ids=true | all-gather | bytes 16896 | tf_op jit(solution)/shard_map/all_gather | solution.py:17
  135.5 0.1 reshape.423
  135.6 87.3 %all-gather.4.cloned.1.call-done = bf16[2048,1152]{1,0:T(8,128)(2,1)} async-done(((bf16[64,1152]{1,0:T(8,128)(2,1)}), bf16[2048,1152]{1,0:T(8,128)(2,1)}) %all-gather.4.cloned.1.call-update) | async-done | bytes 4718608 | tf_op jit(solution)/shard_map/all_gather | solution.py:17
  222.9 2.1 fusion.63
  225.0 3.2 fusion.51
  228.3 0.0 copy-start
  228.3 40.3 %all_to_all.35 = bf16[8,32,2048]{2,1,0:T(8,128)(2,1)S(1)} all-to-all(bf16[8,32,2048]{2,1,0:T(8,128)(2,1)S(1)} %bitcast.136), channel_id=1, replica_groups=mesh['rep'=2,'fs'=32,'tp'=8] {'tp'}, dimensions={0} | all-to-all | bytes 2097152 | tf_op jit(solution)/shard_map/all_to_all | solution.py:51
  268.6 0.1 convert_reduce_fusion.2
  268.8 0.2 multiply_reduce_fusion.2
  269.0 0.1 multiply_convert_fusion.2
  269.1 1.2 broadcast_in_dim.21
  270.3 4.5 all-to-all-start.2
  275.5 14.4 %all-to-all-done.2 = bf16[8,32,2048]{2,1,0:T(8,128)(2,1)S(1)} async-done(((bf16[8,32,2048]{2,1,0:T(8,128)(2,1)}), bf16[8,32,2048]{2,1,0:T(8,128)(2,1)S(1)}, u32[]{:S(2)}, u32[]{:S(2)}) %all-to-all-start.2) | async-done | bytes 1048608 | tf_op jit(solution)/shard_map/all_to_all | solution.py:29
  289.9 1.2 broadcast_in_dim.22
  291.1 11.8 %all-to-all-start.3 = ((bf16[32,256,64]{1,2,0:T(8,128)(2,1)}), bf16[32,256,64]{1,2,0:T(8,128)(2,1)S(1)}, u32[]{:S(2)}, u32[]{:S(2)}) async-start(bf16[32,256,64]{1,2,0:T(8,128)(2,1)} %broadcast_in_dim.22), calls=%async_computation.3 | async-start | bytes 2097152 | tf_op jit(solution)/shard_map/all_to_all | solution.py:29
  302.9 145.8 %all-gather.6.cloned.1.call-done = bf16[2048,768]{1,0:T(8,128)(2,1)} async-done(((bf16[64,768]{1,0:T(8,128)(2,1)}), bf16[2048,768]{1,0:T(8,128)(2,1)}) %all-gather.6.cloned.1.call-update) | async-done | bytes 3145744 | tf_op jit(solution)/shard_map/all_gather | solution.py:57
  448.7 1.7 fusion.92
  450.4 1.7 fusion.93
  452.1 1.7 fusion.94
  453.8 4.5 while.15
  453.8 0.3 fusion.152
  454.2 0.3 fusion.153
  454.4 0.5 fusion.151
  455.0 0.3 fusion.152
  455.3 0.3 fusion.153
  455.5 0.5 fusion.151
  456.1 0.3 fusion.152
  456.4 0.3 fusion.153
  456.7 0.5 fusion.151
  457.2 0.3 fusion.152
  457.5 0.3 fusion.153
  457.8 0.5 fusion.151
  458.3 0.1 reduce_sum.75
  458.4 0.1 div.36
  458.5 0.2 multiply_reduce_fusion.1
  458.7 0.1 rsqrt.38
  458.8 0.5 fusion.50
  459.3 41.5 %all_to_all.36 = bf16[8,32,2048]{2,1,0:T(8,128)(2,1)S(1)} all-to-all(bf16[8,32,2048]{2,1,0:T(8,128)(2,1)S(1)} %bitcast.126), channel_id=1, replica_groups=mesh['rep'=2,'fs'=32,'tp'=8] {'tp'}, dimensions={0} | all-to-all | bytes 2097152 | tf_op jit(solution)/shard_map/all_to_all | solution.py:51
  500.8 0.1 convert_reduce_fusion.1
  500.9 0.2 multiply_reduce_fusion
  501.1 0.1 multiply_convert_fusion
  501.2 0.1 broadcast_in_dim.23
  501.3 18.4 %all_to_all.37 = bf16[8,32,2048]{2,1,0:T(8,128)(2,1)S(1)} all-to-all(bf16[8,32,2048]{2,1,0:T(8,128)(2,1)S(1)} %broadcast_in_dim.23), channel_id=1, replica_groups=mesh['rep'=2,'fs'=32,'tp'=8] {'tp'}, dimensions={0} | all-to-all | bytes 2097152 | tf_op jit(solution)/shard_map/all_to_all | solution.py:29
  519.7 2.1 fusion.66
  521.8 3.3 fusion.52
  525.1 18.4 %all_to_all.38 = bf16[8,32,2048]{2,1,0:T(8,128)(2,1)S(1)} all-to-all(bf16[8,32,2048]{2,1,0:T(8,128)(2,1)S(1)} %bitcast.135), channel_id=1, replica_groups=mesh['rep'=2,'fs'=32,'tp'=8] {'tp'}, dimensions={0} | all-to-all | bytes 2097152 | tf_op jit(solution)/shard_map/all_to_all | solution.py:51
  543.5 0.1 convert_reduce_fusion
  543.7 0.7 add_convert_fusion
  (37 shorter events, 0.2 us)
Async XLA Ops:
  6.5 216.4 %all-gather.4.cloned.1.call-start = ((), (), s32[]{:S(2)}) async-start(), calls=%async_computation.7 | async-start | bytes 4866048 | tf_op jit(solution)/shard_map/all_gather | solution.py:17
  9.9 438.8 %all-gather.6.cloned.1.call-start = ((), (), s32[]{:S(2)}) async-start(), calls=%async_computation.8 | async-start | bytes 3244032 | tf_op jit(solution)/shard_map/all_gather | solution.py:57
  10.8 16.9 %copy-start.3 = (f32[64]{0:T(128)S(1)}, f32[64]{0:T(128)}, u32[]{:S(2)}) copy-start(f32[64]{0:T(128)} %param.35) | copy-start | bytes 772
  10.8 16.9 %copy-start.4 = (f32[64]{0:T(128)S(1)}, f32[64]{0:T(128)}, u32[]{:S(2)}) copy-start(f32[64]{0:T(128)} %param.27) | copy-start | bytes 772
  12.6 210.4 %copy-start.5 = (f32[384]{0:T(512)S(1)}, f32[384]{0:T(512)}, u32[]{:S(2)}) copy-start(f32[384]{0:T(512)} %param.23) | copy-start | bytes 4612
  17.4 118.2 %all-to-all-start = ((bf16[8,32,2048]{2,1,0:T(8,128)(2,1)}), bf16[8,32,2048]{2,1,0:T(8,128)(2,1)S(1)}, u32[]{:S(2)}, u32[]{:S(2)}) async-start(bf16[8,32,2048]{2,1,0:T(8,128)(2,1)} %broadcast_in_dim.17), calls=%async_computation | async-start | bytes 2097152 | tf_op jit(solution)/shard_map/all_to_all | solution.py:29
  27.7 197.4 %copy-start.6 = (f32[384]{0:T(512)S(1)}, f32[384]{0:T(512)}, u32[]{:S(2)}) copy-start(f32[384]{0:T(512)} %param.25) | copy-start | bytes 4612
  228.3 40.5 %copy-start = (bf16[32,2048]{1,0:T(8,128)(2,1)S(1)}, bf16[32,2048]{1,0:T(8,128)(2,1)}, u32[]{:S(2)}) copy-start(bf16[32,2048]{1,0:T(8,128)(2,1)} %param.20) | copy-start | bytes 393220
  268.8 6.7 %copy-start.1 = (f32[256,64]{0,1:T(8,128)S(1)}, f32[256,64]{0,1:T(8,128)}, u32[]{:S(2)}) copy-start(f32[256,64]{0,1:T(8,128)} %param.34) | copy-start | bytes 196612
  270.3 19.6 %all-to-all-start.2 = ((bf16[8,32,2048]{2,1,0:T(8,128)(2,1)}), bf16[8,32,2048]{2,1,0:T(8,128)(2,1)S(1)}, u32[]{:S(2)}, u32[]{:S(2)}) async-start(bf16[8,32,2048]{2,1,0:T(8,128)(2,1)} %broadcast_in_dim.21), calls=%async_computation.2 | async-start | bytes 2097152 | tf_op jit(solution)/shard_map/all_to_all | solution.py:29
  274.8 173.9 %copy-start.7 = (f32[256]{0:T(256)S(1)}, f32[256]{0:T(256)}, u32[]{:S(2)}) copy-start(f32[256]{0:T(256)} %param.31) | copy-start | bytes 3076
  291.1 159.4 %copy-start.8 = (f32[256]{0:T(256)S(1)}, f32[256]{0:T(256)}, u32[]{:S(2)}) copy-start(f32[256]{0:T(256)} %param.33) | copy-start | bytes 3076
  291.1 167.7 %all-to-all-start.3 = ((bf16[32,256,64]{1,2,0:T(8,128)(2,1)}), bf16[32,256,64]{1,2,0:T(8,128)(2,1)S(1)}, u32[]{:S(2)}, u32[]{:S(2)}) async-start(bf16[32,256,64]{1,2,0:T(8,128)(2,1)} %broadcast_in_dim.22), calls=%async_computation.3 | async-start | bytes 2097152 | tf_op jit(solution)/shard_map/all_to_all | solution.py:29
  448.7 3.4 copy-start.9
  453.8 5.0 copy-start.2
Sparse Core Ops, SparseCore 0:
  10.1 212.8 all-gather.3
  225.0 223.6 all-gather.5
where the time goes:
time: 552 us; the launch traced here: 551 us
  waiting for transfers between devices  248 us (45%)
  blocking collectives  226 us (41%)
  starting transfers between devices  26.7 us (5%)
  matrix products  20.6 us (4%)
  between operations  14.4 us (3%)
  other arithmetic  10.7 us (2%)
    all_gather x1, waiting for transfers between devices, in_one_piece(): lax.all_gather(both, axis, axis=dim, tiled=True)  146 us
    all_gather x1, blocking collectives, gather_turned(): result = lax.all_gather(both, axis, axis=0, tiled=True)  108 us
    all_to_all x3, blocking collectives, summed_on_arrival(): lax.all_to_all(blocks, axis, split_axis=0, concat_axis=0, tiled=True)  100 us
    all_gather x1, waiting for transfers between devices, gather_turned(): result = lax.all_gather(both, axis, axis=0, tiled=True)  87.3 us
    all_to_all x3, starting transfers between devices, sent_to_all(): return lax.all_to_all(copies, axis, split_axis=0, concat_axis=0, tiled=True)  26.6 us
    all_to_all x1, blocking collectives, sent_to_all(): return lax.all_to_all(copies, axis, split_axis=0, concat_axis=0, tiled=True)  18.4 us
    all_to_all x3, waiting for transfers between devices, sent_to_all(): return lax.all_to_all(copies, axis, split_axis=0, concat_axis=0, tiled=True)  14.4 us
  transfers between devices with their start and end apart: 5, of which 3 were waited for; matrix products, arithmetic and copies ran while one was open for 5% of the time, Pallas kernels for 0%

commit v1 on v0

--- a/solution.py
+++ b/solution.py
@@ -14,7 +14,8 @@
     turned = [jnp.moveaxis(a, dim, 0) for a, dim in zip(arrays, dims)]
     widths = [t[0].size for t in turned]
     both = jnp.concatenate([t.reshape(-1, w) for t, w in zip(turned, widths)], axis=1)
-    result = lax.all_gather(both, axis, axis=0, tiled=True)
+    repeated = jnp.stack([both] * lax.axis_size(axis))
+    result = jnp.concatenate(lax.all_to_all(repeated, axis, 0, 0), axis=0)
     blocks = jnp.split(result, [sum(widths[:k]) for k in range(1, len(widths))], axis=1)
     return tuple(
         (

time: 552 us -> 483 us (0.88)
  blocking collectives: 226 us -> 79.1 us
  waiting for transfers between devices: 248 us -> 311 us
  starting transfers between devices: 26.7 us -> 42.1 us
    all_to_all x0 -> x2, waiting for transfers between devices: none -> 242 us  [gather_turned(): result = jnp.concatenate(lax.all_to_all(repeated, axis, 0, 0), axis=0)]
    all_gather x1, waiting for transfers between devices: 146 us -> 0.02 us  [in_one_piece(): lax.all_gather(both, axis, axis=dim, tiled=True)]
    all_gather x1 -> x0, blocking collectives: 108 us -> none  [gather_turned(): result = lax.all_gather(both, axis, axis=0, tiled=True)]
    all_gather x1 -> x0, waiting for transfers between devices: 87.3 us -> none  [gather_turned(): result = lax.all_gather(both, axis, axis=0, tiled=True)]
    all_to_all x3, waiting for transfers between devices: 14.4 us -> 68.8 us  [sent_to_all(): return lax.all_to_all(copies, axis, split_axis=0, concat_axis=0, tiled=True)]
    all_to_all x3, blocking collectives: 100 us -> 60.7 us  [summed_on_arrival(): lax.all_to_all(blocks, axis, split_axis=0, concat_axis=0, tiled=True)]
    all_to_all x0 -> x2, starting transfers between devices: none -> 21.1 us  [gather_turned(): result = jnp.concatenate(lax.all_to_all(repeated, axis, 0, 0), axis=0)]
    all_to_all x3, starting transfers between devices: 26.6 us -> 21 us  [sent_to_all(): return lax.all_to_all(copies, axis, split_axis=0, concat_axis=0, tiled=True)]
  transfers between devices with their start and end apart: 5 -> 6, of which waited for: 3 -> 5; matrix products, arithmetic and copies ran while one was open for 5% -> 5% of each run, Pallas kernels for 0% -> 0%
where the time goes in v1:
time: 483 us; the launch traced here: 482 us
  waiting for transfers between devices  311 us (64%)
  blocking collectives  79.1 us (16%)
  starting transfers between devices  42.1 us (9%)
  matrix products  20.5 us (4%)
  between operations  14.5 us (3%)
  local copies, waits for them, and re-layouts  8.81 us (2%)
  other arithmetic  6.1 us (1%)
    all_to_all x2, waiting for transfers between devices, gather_turned(): result = jnp.concatenate(lax.all_to_all(repeated, axis, 0, 0), axis=0)  242 us
    all_to_all x3, waiting for transfers between devices, sent_to_all(): return lax.all_to_all(copies, axis, split_axis=0, concat_axis=0, tiled=True)  68.8 us
    all_to_all x3, blocking collectives, summed_on_arrival(): lax.all_to_all(blocks, axis, split_axis=0, concat_axis=0, tiled=True)  60.7 us
    all_to_all x2, starting transfers between devices, gather_turned(): result = jnp.concatenate(lax.all_to_all(repeated, axis, 0, 0), axis=0)  21.1 us
    all_to_all x3, starting transfers between devices, sent_to_all(): return lax.all_to_all(copies, axis, split_axis=0, concat_axis=0, tiled=True)  21 us
    all_to_all x1, blocking collectives, sent_to_all(): return lax.all_to_all(copies, axis, split_axis=0, concat_axis=0, tiled=True)  18.4 us
  transfers between devices with their start and end apart: 6, of which 5 were waited for; matrix products, arithmetic and copies ran while one was open for 5% of the time, Pallas kernels for 0%

profile of v1, /device:TPU:1, one launch (start us, length us, event | category | flops | bytes accessed | tf_op | source)
XLA Modules:
  0.0 482.1 jit_solution(14007644322571207614)
XLA Ops:
  6.5 0.7 pad_maximum_fusion.2
  7.3 0.7 reshape.455
  8.0 16.1 %all-to-all-start.2 = ((f32[32,1,128]{2,1,0:T(1,128)}), f32[32,1,128]{2,1,0:T(1,128)S(1)}, u32[]{:S(2)}, u32[]{:S(2)}) async-start(f32[32,1,128]{2,1,0:T(1,128)} %reshape.455), calls=%async_computation.2 | async-start | bytes 32768 | tf_op jit(solution)/shard_map/all_to_all | solution.py:18
  24.1 0.9 fusion.124
  25.0 1.0 fusion.108
  26.0 1.0 fusion.110
  27.0 8.4 %all-to-all-done.2 = f32[32,1,128]{2,1,0:T(1,128)S(1)} async-done(((f32[32,1,128]{2,1,0:T(1,128)}), f32[32,1,128]{2,1,0:T(1,128)S(1)}, u32[]{:S(2)}, u32[]{:S(2)}) %all-to-all-start.2) | async-done | bytes 16416 | tf_op jit(solution)/shard_map/all_to_all | solution.py:18
  35.5 1.1 broadcast_in_dim.17
  36.5 6.4 %all-to-all-start = ((bf16[8,32,2048]{2,1,0:T(8,128)(2,1)}), bf16[8,32,2048]{2,1,0:T(8,128)(2,1)S(1)}, u32[]{:S(2)}, u32[]{:S(2)}) async-start(bf16[8,32,2048]{2,1,0:T(8,128)(2,1)} %broadcast_in_dim.17), calls=%async_computation | async-start | bytes 2097152 | tf_op jit(solution)/shard_map/all_to_all | solution.py:30
  43.0 14.9 %all-to-all-done = bf16[8,32,2048]{2,1,0:T(8,128)(2,1)S(1)} async-done(((bf16[8,32,2048]{2,1,0:T(8,128)(2,1)}), bf16[8,32,2048]{2,1,0:T(8,128)(2,1)S(1)}, u32[]{:S(2)}, u32[]{:S(2)}) %all-to-all-start) | async-done | bytes 1048608 | tf_op jit(solution)/shard_map/all_to_all | solution.py:30
  57.9 2.8 stack.4
  60.7 5.0 %all-to-all-start.1 = ((bf16[32,64,1152]{2,1,0:T(8,128)(2,1)}), bf16[32,64,1152]{2,1,0:T(8,128)(2,1)}, u32[]{:S(2)}, u32[]{:S(2)}) async-start(bf16[32,64,1152]{2,1,0:T(8,128)(2,1)} %stack.4), calls=%async_computation.1 | async-start | bytes 9437184 | tf_op jit(solution)/shard_map/all_to_all | solution.py:18
  65.7 0.0 all-gather.2.cloned.1.call-start
  65.9 0.6 pad_maximum_fusion.1
  66.5 0.5 broadcast.260
  67.0 0.6 reduce.5
  67.6 0.1 reshape.456
  67.7 0.1 reshape.425
  67.8 233.5 %all-to-all-done.1 = bf16[32,64,1152]{2,1,0:T(8,128)(2,1)} async-done(((bf16[32,64,1152]{2,1,0:T(8,128)(2,1)}), bf16[32,64,1152]{2,1,0:T(8,128)(2,1)}, u32[]{:S(2)}, u32[]{:S(2)}) %all-to-all-start.1) | async-done | bytes 4718624 | tf_op jit(solution)/shard_map/all_to_all | solution.py:18
  301.3 2.1 fusion.63
  303.5 3.2 fusion.51
  306.7 21.9 %all_to_all.45 = bf16[8,32,2048]{2,1,0:T(8,128)(2,1)S(1)} all-to-all(bf16[8,32,2048]{2,1,0:T(8,128)(2,1)S(1)} %bitcast.138), channel_id=1, replica_groups=mesh['rep'=2,'fs'=32,'tp'=8] {'tp'}, dimensions={0} | all-to-all | bytes 2097152 | tf_op jit(solution)/shard_map/all_to_all | solution.py:52
  328.6 0.1 convert_reduce_fusion.2
  328.8 0.2 multiply_reduce_fusion.2
  328.9 0.1 multiply_convert_fusion.2
  329.0 1.1 broadcast_in_dim.21
  330.2 4.5 all-to-all-start.4
  335.4 14.3 %all-to-all-done.4 = bf16[8,32,2048]{2,1,0:T(8,128)(2,1)S(1)} async-done(((bf16[8,32,2048]{2,1,0:T(8,128)(2,1)}), bf16[8,32,2048]{2,1,0:T(8,128)(2,1)S(1)}, u32[]{:S(2)}, u32[]{:S(2)}) %all-to-all-start.4) | async-done | bytes 1048608 | tf_op jit(solution)/shard_map/all_to_all | solution.py:30
  349.7 1.1 broadcast_in_dim.22
  350.8 10.1 %all-to-all-start.5 = ((bf16[32,256,64]{1,2,0:T(8,128)(2,1)}), bf16[32,256,64]{1,2,0:T(8,128)(2,1)S(1)}, u32[]{:S(2)}, u32[]{:S(2)}) async-start(bf16[32,256,64]{1,2,0:T(8,128)(2,1)} %broadcast_in_dim.22), calls=%async_computation.5 | async-start | bytes 2097152 | tf_op jit(solution)/shard_map/all_to_all | solution.py:30
  360.9 0.0 all-gather.2.cloned.1.call-done
  361.0 1.7 fusion.92
  362.7 1.7 fusion.93
  364.4 1.7 fusion.94
  366.1 4.5 while.15
  366.1 0.3 fusion.152
  366.4 0.3 fusion.153
  366.7 0.5 fusion.151
  367.2 0.3 fusion.152
  367.5 0.3 fusion.153
  367.8 0.5 fusion.151
  368.3 0.3 fusion.152
  368.6 0.3 fusion.153
  368.9 0.5 fusion.151
  369.4 0.3 fusion.152
  369.7 0.3 fusion.153
  370.0 0.5 fusion.151
  370.5 0.1 reduce_sum.75
  370.6 0.1 div.36
  370.7 0.2 multiply_reduce_fusion.1
  370.9 0.1 rsqrt.38
  371.0 39.7 %all-to-all-done.5 = bf16[32,256,64]{1,2,0:T(8,128)(2,1)S(1)} async-done(((bf16[32,256,64]{1,2,0:T(8,128)(2,1)}), bf16[32,256,64]{1,2,0:T(8,128)(2,1)S(1)}, u32[]{:S(2)}, u32[]{:S(2)}) %all-to-all-start.5) | async-done | bytes 1048608 | tf_op jit(solution)/shard_map/all_to_all | solution.py:30
  410.7 0.5 fusion.50
  411.2 20.4 %all_to_all.46 = bf16[8,32,2048]{2,1,0:T(8,128)(2,1)S(1)} all-to-all(bf16[8,32,2048]{2,1,0:T(8,128)(2,1)S(1)} %bitcast.128), channel_id=1, replica_groups=mesh['rep'=2,'fs'=32,'tp'=8] {'tp'}, dimensions={0} | all-to-all | bytes 2097152 | tf_op jit(solution)/shard_map/all_to_all | solution.py:52
  431.6 0.1 convert_reduce_fusion.1
  431.8 0.2 multiply_reduce_fusion
  432.0 0.1 multiply_convert_fusion
  432.1 0.1 broadcast_in_dim.23
  432.2 18.4 %all_to_all.47 = bf16[8,32,2048]{2,1,0:T(8,128)(2,1)S(1)} all-to-all(bf16[8,32,2048]{2,1,0:T(8,128)(2,1)S(1)} %broadcast_in_dim.23), channel_id=1, replica_groups=mesh['rep'=2,'fs'=32,'tp'=8] {'tp'}, dimensions={0} | all-to-all | bytes 2097152 | tf_op jit(solution)/shard_map/all_to_all | solution.py:30
  450.6 2.1 fusion.66
  452.7 3.3 fusion.52
  456.0 18.4 %all_to_all.48 = bf16[8,32,2048]{2,1,0:T(8,128)(2,1)S(1)} all-to-all(bf16[8,32,2048]{2,1,0:T(8,128)(2,1)S(1)} %bitcast.137), channel_id=1, replica_groups=mesh['rep'=2,'fs'=32,'tp'=8] {'tp'}, dimensions={0} | all-to-all | bytes 2097152 | tf_op jit(solution)/shard_map/all_to_all | solution.py:52
  474.4 0.1 convert_reduce_fusion
  474.5 0.7 add_convert_fusion
  (51 shorter events, 0.3 us)
Async XLA Ops:
  6.5 36.4 %copy-start.1 = (f32[64,384]{1,0:T(8,128)S(1)}, f32[64,384]{1,0:T(8,128)}, u32[]{:S(2)}) copy-start(f32[64,384]{1,0:T(8,128)} %param.22) | copy-start | bytes 294916
  6.5 36.4 %copy-start.2 = (f32[64,384]{1,0:T(8,128)S(1)}, f32[64,384]{1,0:T(8,128)}, u32[]{:S(2)}) copy-start(f32[64,384]{1,0:T(8,128)} %param.24) | copy-start | bytes 294916
  6.5 36.5 %copy-start.3 = (f32[384,64]{0,1:T(8,128)S(1)}, f32[384,64]{0,1:T(8,128)}, u32[]{:S(2)}) copy-start(f32[384,64]{0,1:T(8,128)} %param.26) | copy-start | bytes 294916
  8.0 27.5 %all-to-all-start.2 = ((f32[32,1,128]{2,1,0:T(1,128)}), f32[32,1,128]{2,1,0:T(1,128)S(1)}, u32[]{:S(2)}, u32[]{:S(2)}) async-start(f32[32,1,128]{2,1,0:T(1,128)} %reshape.455), calls=%async_computation.2 | async-start | bytes 32768 | tf_op jit(solution)/shard_map/all_to_all | solution.py:18
  36.5 21.4 %all-to-all-start = ((bf16[8,32,2048]{2,1,0:T(8,128)(2,1)}), bf16[8,32,2048]{2,1,0:T(8,128)(2,1)S(1)}, u32[]{:S(2)}, u32[]{:S(2)}) async-start(bf16[8,32,2048]{2,1,0:T(8,128)(2,1)} %broadcast_in_dim.17), calls=%async_computation | async-start | bytes 2097152 | tf_op jit(solution)/shard_map/all_to_all | solution.py:30
  60.7 5.1 %copy-start.4 = (f32[64,256]{1,0:T(8,128)S(1)}, f32[64,256]{1,0:T(8,128)}, u32[]{:S(2)}) copy-start(f32[64,256]{1,0:T(8,128)} %param.28) | copy-start | bytes 196612
  60.7 5.1 %copy-start.5 = (f32[64,256]{1,0:T(8,128)S(1)}, f32[64,256]{1,0:T(8,128)}, u32[]{:S(2)}) copy-start(f32[64,256]{1,0:T(8,128)} %param.30) | copy-start | bytes 196612
  60.7 5.1 %copy-start.6 = (f32[64,256]{1,0:T(8,128)S(1)}, f32[64,256]{1,0:T(8,128)}, u32[]{:S(2)}) copy-start(f32[64,256]{1,0:T(8,128)} %param.32) | copy-start | bytes 196612
  60.7 240.6 %copy-start.9 = (f32[384]{0:T(512)S(1)}, f32[384]{0:T(512)}, u32[]{:S(2)}) copy-start(f32[384]{0:T(512)} %param.23) | copy-start | bytes 4612
  60.7 240.6 %all-to-all-start.1 = ((bf16[32,64,1152]{2,1,0:T(8,128)(2,1)}), bf16[32,64,1152]{2,1,0:T(8,128)(2,1)}, u32[]{:S(2)}, u32[]{:S(2)}) async-start(bf16[32,64,1152]{2,1,0:T(8,128)(2,1)} %stack.4), calls=%async_computation.1 | async-start | bytes 9437184 | tf_op jit(solution)/shard_map/all_to_all | solution.py:18
  65.7 295.2 %all-gather.2.cloned.1.call-start = ((), (), s32[]{:S(2)}) async-start(), calls=%async_computation.9 | async-start | bytes 3244032 | tf_op jit(solution)/shard_map/all_gather | solution.py:58
  65.9 237.6 %copy-start.10 = (f32[384]{0:T(512)S(1)}, f32[384]{0:T(512)}, u32[]{:S(2)}) copy-start(f32[384]{0:T(512)} %param.25) | copy-start | bytes 4612
  306.7 22.0 %copy-start = (bf16[32,2048]{1,0:T(8,128)(2,1)S(1)}, bf16[32,2048]{1,0:T(8,128)(2,1)}, u32[]{:S(2)}) copy-start(bf16[32,2048]{1,0:T(8,128)(2,1)} %param.20) | copy-start | bytes 393220
  328.8 6.6 %copy-start.7 = (f32[256,64]{0,1:T(8,128)S(1)}, f32[256,64]{0,1:T(8,128)}, u32[]{:S(2)}) copy-start(f32[256,64]{0,1:T(8,128)} %param.34) | copy-start | bytes 196612
  330.2 19.5 %all-to-all-start.4 = ((bf16[8,32,2048]{2,1,0:T(8,128)(2,1)}), bf16[8,32,2048]{2,1,0:T(8,128)(2,1)S(1)}, u32[]{:S(2)}, u32[]{:S(2)}) async-start(bf16[8,32,2048]{2,1,0:T(8,128)(2,1)} %broadcast_in_dim.21), calls=%async_computation.4 | async-start | bytes 2097152 | tf_op jit(solution)/shard_map/all_to_all | solution.py:30
  334.7 26.3 %copy-start.11 = (f32[256]{0:T(256)S(1)}, f32[256]{0:T(256)}, u32[]{:S(2)}) copy-start(f32[256]{0:T(256)} %param.31) | copy-start | bytes 3076
  350.8 11.8 %copy-start.12 = (f32[256]{0:T(256)S(1)}, f32[256]{0:T(256)}, u32[]{:S(2)}) copy-start(f32[256]{0:T(256)} %param.33) | copy-start | bytes 3076
  350.8 59.9 %all-to-all-start.5 = ((bf16[32,256,64]{1,2,0:T(8,128)(2,1)}), bf16[32,256,64]{1,2,0:T(8,128)(2,1)S(1)}, u32[]{:S(2)}, u32[]{:S(2)}) async-start(bf16[32,256,64]{1,2,0:T(8,128)(2,1)} %broadcast_in_dim.22), calls=%async_computation.5 | async-start | bytes 2097152 | tf_op jit(solution)/shard_map/all_to_all | solution.py:30
  361.0 3.4 copy-start.13
  366.0 44.7 %copy-start.8 = (f32[256]{0:T(256)S(1)}, f32[256]{0:T(256)}, u32[]{:S(2)}) copy-start(f32[256]{0:T(256)} %param.36) | copy-start | bytes 3076
Sparse Core Ops, SparseCore 0:
  68.6 215.4 all-gather.1
